TPU v7x, 32 devices: a whole 2x2x4 slice. The times are simulated.
32 devices in a mesh: ep: 8 (over z, y), tp: 4 (over x, core).
Axes of the slice: x: 2, y: 2, z: 4, core: 2. Of those that a mesh axis runs over, the one named last changes fastest.
Arguments:
- queries: bfloat16 [1536, 2048], P('ep', 'tp'), may hold values from -5 to 5
- keys: bfloat16 [1536, 512], P('ep', 'tp'), may hold values from -5 to 5
- values: bfloat16 [1536, 512], P('ep', 'tp'), may hold values from -6 to 6
- query_gain: float32 [128], replicated, may hold values from 0.6 to 6
- key_gain: float32 [128], replicated, may hold values from 0.6 to 6
- out_weight: bfloat16 [2048, 2048], P('tp'), may hold values from -0.125 to 0.125
- mixer_gain: float32 [2048], replicated, may hold values from 0.1 to 1.9
- expert_in: bfloat16 [4096, 2048], P(('ep', 'tp')), may hold values from -6 to 6
- routes: int32 [4096, 2], P(('ep', 'tp')), may hold values from 0 to 7, all different within a row; in each aligned block of 128 rows (0 to 127, 128 to 255, ...) at most 48 rows name the same one
- route_weights: float32 [4096, 2], P(('ep', 'tp')), may hold values from 0.2 to 1
- expert_gain: float32 [2048], replicated, may hold values from 0.5 to 4
- gate_w: bfloat16 [8, 2048, 2048], P('ep', None, 'tp'), may hold values from -0.125 to 0.125
- up_w: bfloat16 [8, 2048, 2048], P('ep', None, 'tp'), may hold values from -0.125 to 0.125
- down_w: bfloat16 [8, 2048, 2048], P('ep', 'tp'), may hold values from -0.125 to 0.125
- ffn_out_gain: float32 [2048], replicated, may hold values from 0.1 to 1.9
Outputs:
- mixer_out: bfloat16 [1536, 2048], P(('ep', 'tp'))
- expert_out: bfloat16 [4096, 2048], P(('ep', 'tp'))
Inputs may be any that keep to these rules, and one draw needn't show every extreme that they name: `routes`: each row names 2 different experts. Among the rows of one device no expert is named by more than 48 rows, and in every draw some expert is named by exactly 48 rows of some device.
All inputs are finite; a program needn't handle non-finite values.
Results may differ from a plain program's by a relative error of at most 0.015.
The roundings to bfloat16 on the way count: a program that leaves them out, or rounds other values in their place, can miss the bound.
Values may be sent and summed in bfloat16 or wider, within the bound.
No kernel may reach another device: no remote copies, remote signals or barrier semaphores. Data moves between devices by JAX's collectives and lax.ppermute only.
A program may use at most 128 MiB of HBM per device.

v0:
```python
import jax
import jax.numpy as jnp
from jax import lax
from jax.sharding import PartitionSpec as P

HEAD = 128
GRID_W = 64
norm_eps = 1e-06
rope_base = 10000.0
clamp_limit = 7.0
sigmoid_slope = 1.702


def rms_scale(values_in, gain):
    return (
        values_in
        * lax.rsqrt(jnp.mean(values_in * values_in, axis=-1, keepdims=True) + norm_eps)
        * gain
    )


def turn_pair(halfpart, cosine, sine):
    first_part, second_part = jnp.split(halfpart, 2, axis=-1)
    return jnp.concatenate(
        [first_part * cosine - second_part * sine, second_part * cosine + first_part * sine],
        axis=-1,
    )


def grid_rotate(field, position):
    half_width = field.shape[-1] // 2
    inverse = rope_base ** (-jnp.arange(0, half_width, 2, dtype=jnp.float32) / half_width)
    grid_row = (position // GRID_W).astype(jnp.float32)
    grid_col = (position % GRID_W).astype(jnp.float32)
    row_angle = (grid_row[:, None] * inverse[None, :])[:, None, :]
    col_angle = (grid_col[:, None] * inverse[None, :])[:, None, :]
    return jnp.concatenate(
        [
            turn_pair(field[..., :half_width], jnp.cos(row_angle), jnp.sin(row_angle)),
            turn_pair(field[..., half_width:], jnp.cos(col_angle), jnp.sin(col_angle)),
        ],
        axis=-1,
    )


def clamped_unit(gate_pre, up_pre):
    gate_cut = jnp.minimum(gate_pre, clamp_limit)
    up_cut = jnp.clip(up_pre, -clamp_limit, clamp_limit)
    return ((up_cut + 1.0) * gate_cut * jax.nn.sigmoid(sigmoid_slope * gate_cut)).astype(
        jnp.bfloat16
    )


def mixer_half(queries, keys, values, query_gain, key_gain, out_weight, mixer_gain):
    local_rows = queries.shape[0]
    kv_local = keys.shape[1] // HEAD
    group_size = queries.shape[1] // HEAD // kv_local
    position = lax.axis_index("ep") * local_rows + jnp.arange(local_rows, dtype=jnp.int32)
    query_f = queries.astype(jnp.float32).reshape(local_rows, kv_local * group_size, HEAD)
    query_norm = grid_rotate(rms_scale(query_f, query_gain), position).astype(jnp.bfloat16)
    query_norm = query_norm.reshape(local_rows, kv_local, group_size, HEAD)
    key_f = keys.astype(jnp.float32).reshape(local_rows, kv_local, HEAD)
    key_norm = grid_rotate(rms_scale(key_f, key_gain), position).astype(jnp.bfloat16)
    key_norm = key_norm.reshape(local_rows, kv_local * HEAD)
    score_scale = HEAD ** (-0.5)
    initial = (
        jnp.full((kv_local, group_size, local_rows), -1e30, jnp.float32),
        jnp.zeros((kv_local, group_size, local_rows), jnp.float32),
        jnp.zeros((kv_local, group_size, local_rows, HEAD), jnp.float32),
    )
    key_piece = lax.all_gather(key_norm, "ep", axis=0, tiled=True)
    value_piece = lax.all_gather(values, "ep", axis=0, tiled=True)
    piece_rows = key_piece.shape[0]
    block_rows = 1
    for candidate in range(min(piece_rows, 1024), 0, -1):
        if piece_rows % candidate == 0:
            block_rows = candidate
            break
    key_blocks = key_piece.reshape(piece_rows // block_rows, block_rows, kv_local, HEAD)
    value_blocks = value_piece.reshape(piece_rows // block_rows, block_rows, kv_local, HEAD)

    def one_block(state, blocks_in):
        running_max, running_total, weighted = state
        key_block, value_block = blocks_in
        scores = (
            jnp.einsum("qhgd,khd->hgqk", query_norm, key_block, preferred_element_type=jnp.float32)
            * score_scale
        )
        new_max = jnp.maximum(running_max, jnp.max(scores, axis=-1))
        factor = jnp.exp(running_max - new_max)
        expo = jnp.exp(scores - new_max[..., None])
        new_total = running_total * factor + jnp.sum(expo, axis=-1)
        new_weighted = weighted * factor[..., None] + jnp.einsum(
            "hgqk,khd->hgqd",
            expo.astype(jnp.bfloat16),
            value_block,
            preferred_element_type=jnp.float32,
        )
        return ((new_max, new_total, new_weighted), None)

    state_out, unused = lax.scan(one_block, initial, (key_blocks, value_blocks))
    final_max, final_total, weighted = state_out
    attended = (weighted / final_total[..., None]).astype(jnp.bfloat16)
    attended = jnp.transpose(attended, (2, 0, 1, 3)).reshape(
        local_rows, kv_local * group_size * HEAD
    )
    share_rows = local_rows // lax.axis_size("tp")
    selected = lax.slice_in_dim(attended, 0, lax.axis_size("tp") * share_rows, axis=0)
    projected = lax.psum_scatter(
        jnp.dot(selected, out_weight, preferred_element_type=jnp.float32).astype(jnp.bfloat16),
        "tp",
        scatter_dimension=0,
        tiled=True,
    ).astype(jnp.float32)
    return rms_scale(projected, mixer_gain).astype(jnp.bfloat16)


def expert_half(expert_in, routes, route_weights, expert_gain, gate_w, up_w, down_w, ffn_out_gain):
    tok_rows = expert_in.shape[0]
    model_width = expert_in.shape[1]
    top_count = routes.shape[1]
    expert_count = lax.axis_size("ep")
    capacity = max(2, (3 * tok_rows * top_count + 2 * expert_count - 1) // (2 * expert_count))
    normed = rms_scale(expert_in.astype(jnp.float32), expert_gain).astype(jnp.bfloat16)
    pair_expert = routes.reshape(-1)
    pair_count = pair_expert.shape[0]
    one_hot = (pair_expert[:, None] == jnp.arange(expert_count, dtype=jnp.int32)[None, :]).astype(
        jnp.int32
    )
    pair_rank = jnp.sum(jnp.cumsum(one_hot, axis=0) * one_hot, axis=1) - 1
    pair_slot = pair_expert * capacity + pair_rank
    slot_pair = (
        jnp.full((expert_count * capacity,), pair_count, jnp.int32)
        .at[pair_slot]
        .set(jnp.arange(pair_count, dtype=jnp.int32))
    )
    padded = jnp.concatenate([normed, jnp.zeros((1, model_width), jnp.bfloat16)], axis=0)
    outgoing = padded[slot_pair // top_count].reshape(expert_count, capacity, model_width)
    gate_local = gate_w[0]
    up_local = up_w[0]
    down_local = down_w[0]
    arrived = lax.all_to_all(outgoing, "ep", split_axis=0, concat_axis=0, tiled=True)
    flat_rows = arrived.reshape(-1, model_width)
    shard_rows = lax.all_gather(flat_rows, "tp", axis=0, tiled=True)
    hidden = clamped_unit(
        jnp.dot(shard_rows, gate_local, preferred_element_type=jnp.float32),
        jnp.dot(shard_rows, up_local, preferred_element_type=jnp.float32),
    )
    selected = lax.slice_in_dim(hidden, 0, lax.axis_size("tp") * flat_rows.shape[0], axis=0)
    result = lax.psum_scatter(
        jnp.dot(selected, down_local, preferred_element_type=jnp.float32).astype(jnp.bfloat16),
        "tp",
        scatter_dimension=0,
        tiled=True,
    )
    finished = result.reshape(arrived.shape)
    returned = lax.all_to_all(finished, "ep", split_axis=0, concat_axis=0, tiled=True)
    pair_result = returned.reshape(-1, model_width)[pair_slot].reshape(
        tok_rows, top_count, model_width
    )
    combined = jnp.einsum("tk,tkd->td", route_weights, pair_result.astype(jnp.float32))
    return rms_scale(combined, ffn_out_gain).astype(jnp.bfloat16)


def local(
    queries,
    keys,
    values,
    query_gain,
    key_gain,
    out_weight,
    mixer_gain,
    expert_in,
    routes,
    route_weights,
    expert_gain,
    gate_w,
    up_w,
    down_w,
    ffn_out_gain,
):
    mixer_out = mixer_half(queries, keys, values, query_gain, key_gain, out_weight, mixer_gain)
    expert_out = expert_half(
        expert_in, routes, route_weights, expert_gain, gate_w, up_w, down_w, ffn_out_gain
    )
    return (mixer_out, expert_out)


def solution(mesh):
    in_specs = (
        P("ep", "tp"),
        P("ep", "tp"),
        P("ep", "tp"),
        P(),
        P(),
        P("tp", None),
        P(),
        P(("ep", "tp"), None),
        P(("ep", "tp"), None),
        P(("ep", "tp"), None),
        P(),
        P("ep", None, "tp"),
        P("ep", None, "tp"),
        P("ep", "tp", None),
        P(),
    )
    out_specs = (P(("ep", "tp"), None), P(("ep", "tp"), None))
    return jax.shard_map(local, mesh=mesh, in_specs=in_specs, out_specs=out_specs, check_vma=False)
```

profile of v0, /device:TPU:0, one launch (start us, length us, event | category | flops | bytes accessed | tf_op | source)
XLA Modules:
  0.0 257.0 jit_solution(10198125140260231767)
XLA Ops:
  10.3 1.4 scatter_custom_fusion
  11.8 1.2 fusion.25
  13.0 1.2 fusion.27
  14.3 3.1 %gather_fusion = bf16[384,2048]{1,0:T(8,128)(2,1)} fusion(bf16[129,2048]{1,0:T(8,128)(2,1)S(1)} %concatenate.47, s32[1024]{0:T(1024)S(1)} %pad_clamp_fusion.1), kind=kCustom, calls=%fused_computation | custom fusion | bytes 3147264 | tf_op jit(solution)/shard_map/gather | solution.py:138
  17.4 44.4 %all_to_all.10 = bf16[8,48,2048]{2,1,0:T(8,128)(2,1)} all-to-all(bf16[8,48,2048]{2,1,0:T(8,128)(2,1)} %bitcast.136), channel_id=1, replica_groups=mesh['ep'=8,'tp'=4] {'ep'}, dimensions={0} | all-to-all | bytes 3145728 | tf_op jit(solution)/shard_map/all_to_all | solution.py:142
  62.1 45.3 %all-gather.2.cloned.1.call-done = bf16[1536,2048]{1,0:T(8,128)(2,1)} async-done(((bf16[384,2048]{1,0:T(8,128)(2,1)}), bf16[1536,2048]{1,0:T(8,128)(2,1)}) %all-gather.2.cloned.1.call-update) | async-done | bytes 6291472 | tf_op jit(solution)/shard_map/all_gather | solution.py:144
  107.4 8.5 %convolution_minimum_fusion = f32[1536,512]{1,0:T(8,128)} fusion(bf16[1536,2048]{1,0:T(8,128)(2,1)} %all-gather.2.cloned.1.call-done, bf16[1,2048,512]{2,1,0:T(8,128)(2,1)} %param.28), kind=kOutput, calls=%fused_computation.30 | convolution fusion | flops 3222011904 | bytes 11534336 | tf_op jit(solution)/shard_map/dot_general | solution.py:146
  115.9 11.9 %convolution_convert_fusion = bf16[1536,2048]{1,0:T(8,128)(2,1)} fusion(bf16[1,512,2048]{2,1,0:T(8,128)(2,1)S(1)} %copy-done, f32[1536,512]{1,0:T(8,128)} %convolution_minimum_fusion, bf16[1536,2048]{1,0:T(8,128)(2,1)} %all-gather.2.cloned.1.call-done, bf16[1,2048,512]{2,1,0:T(8,128)(2,1)} %param.29), kind=kOutput, calls=%fused_computation.28 | convolution fusion | flops 6452674560 | bytes 19922944 | tf_op jit(solution)/shard_map/dot_general | solution.py:151
  132.9 31.2 %all_gather.9 = bf16[1536,128]{1,0:T(8,128)(2,1)S(1)} all-gather(bf16[192,128]{1,0:T(8,128)(2,1)S(1)} %pad_maximum_fusion.1), channel_id=1, replica_groups=mesh['ep'=8,'tp'=4] {'ep'}, dimensions={0}, use_global_device_ids=true | all-gather | bytes 442368 | tf_op jit(solution)/shard_map/all_gather | solution.py:71
  164.1 31.0 %all_gather.10 = bf16[1536,128]{1,0:T(8,128)(2,1)S(1)} all-gather(bf16[192,128]{1,0:T(8,128)(2,1)S(1)} %copy-done.4), channel_id=1, replica_groups=mesh['ep'=8,'tp'=4] {'ep'}, dimensions={0}, use_global_device_ids=true | all-gather | bytes 442368 | tf_op jit(solution)/shard_map/all_gather | solution.py:72
  195.1 10.1 %while.15 = (s32[]{:T(128)}, f32[1,4,192]{2,1,0:T(4,128)S(1)}, f32[1,4,192]{2,1,0:T(4,128)S(1)}, f32[1,4,192,128]{3,2,1,0:T(8,128)S(1)}, bf16[2,768,1,128]{3,1,2...) while((s32[]{:T(128)}, f32[1,4,192]{2,1,0:T(4,128)S(1)}, ...), condition=%wide.region_5.6_spmd.clone, body=%wide.region_2.5_spmd.clone.sunk | while | flops 307008000 | bytes 17942668 | solution.py:101
  195.1 1.9 bitcast_reduce_fusion.2
  197.0 2.5 fusion.94
  200.1 1.9 bitcast_reduce_fusion.2
  202.0 2.5 fusion.94
  205.2 5.6 %all-to-all-start.1 = ((bf16[8,48,2048]{2,1,0:T(8,128)(2,1)}), bf16[8,48,2048]{2,1,0:T(8,128)(2,1)}, u32[]{:S(2)}, u32[]{:S(2)}) async-start(bf16[8,48,2048]{2,1,0:T(8,128)(2,1)} %bitcast.141), calls=%async_computation.3 | async-start | bytes 3145728 | tf_op jit(solution)/shard_map/all_to_all | solution.py:157
  211.4 3.1 %convolution_convert_fusion.1 = bf16[192,2048]{1,0:T(8,128)(2,1)} fusion(bf16[512,2048]{1,0:T(8,128)(2,1)} %param.22, bf16[24,8,4,128]{3,2,1,0:T(4,128)(2,1)S(1)} %bitcast.142), kind=kOutput, calls=%fused_computation.35 | convolution fusion | flops 403046400 | bytes 3080192 | tf_op jit(solution)/shard_map/dot_general | solution.py:110
  214.7 23.4 %reduce-scatter.3.cloned.1.call-done = bf16[48,2048]{1,0:T(8,128)(2,1)} async-done(((bf16[192,2048]{1,0:T(8,128)(2,1)}), bf16[48,2048]{1,0:T(8,128)(2,1)}) %reduce-scatter.3.cloned.1.call-update) | async-done | bytes 196624 | tf_op jit(solution)/shard_map/reduce_scatter | solution.py:109
  238.1 1.1 fusion.33
  239.2 1.7 fusion.35
  240.9 4.0 %gather_fusion.1 = bf16[256,2048]{1,0:T(8,128)(2,1)S(1)} fusion(bf16[384,2048]{1,0:T(8,128)(2,1)} %bitcast.23, s32[1024]{0:T(1024)S(1)} %pad_clamp_fusion), kind=kCustom, calls=%fused_computation.1 | custom fusion | bytes 2098176 | tf_op jit(solution)/shard_map/gather | solution.py:158
  244.9 1.5 reshape.497
  246.4 2.5 fusion.79
  249.3 1.2 fusion.30
  (82 shorter events, 10.8 us)
Async XLA Ops:
  7.2 108.7 %copy-start = (bf16[1,512,2048]{2,1,0:T(8,128)(2,1)S(1)}, bf16[1,512,2048]{2,1,0:T(8,128)(2,1)}, u32[]{:S(2)}) copy-start(bf16[1,512,2048]{2,1,0:T(8,128)(2,1)} %param.30) | copy-start | bytes 6291460
  7.2 100.2 %all-gather.2.cloned.1.call-start = ((), (), s32[]{:S(2)}) async-start(), calls=%async_computation.5 | async-start | bytes 7864320 | tf_op jit(solution)/shard_map/all_gather | solution.py:144
  61.9 143.3 %reduce-scatter.5.cloned.1.call-start = ((), (), s32[]{:S(2)}) async-start(), calls=%async_computation.6 | async-start | bytes 7864320 | tf_op jit(solution)/shard_map/reduce_scatter | solution.py:150
  127.8 0.9 copy-start.3
  127.9 2.2 copy-start.8
  130.0 1.7 copy-start.2
  130.0 1.8 copy-start.9
  130.3 33.7 %copy-start.4 = (bf16[192,128]{1,0:T(8,128)(2,1)S(1)}, bf16[192,128]{1,0:T(8,128)(2,1)}, u32[]{:S(2)}) copy-start(bf16[192,128]{1,0:T(8,128)(2,1)} %param.19) | copy-start | bytes 147460
  197.0 2.5 copy-start.1
  202.0 2.5 copy-start.1
  205.2 35.7 %all-to-all-start.1 = ((bf16[8,48,2048]{2,1,0:T(8,128)(2,1)}), bf16[8,48,2048]{2,1,0:T(8,128)(2,1)}, u32[]{:S(2)}, u32[]{:S(2)}) async-start(bf16[8,48,2048]{2,1,0:T(8,128)(2,1)} %bitcast.141), calls=%async_computation.3 | async-start | bytes 3145728 | tf_op jit(solution)/shard_map/all_to_all | solution.py:157
  210.8 27.3 %reduce-scatter.3.cloned.1.call-start = ((), (), s32[]{:S(2)}) async-start(), calls=%async_computation.4 | async-start | bytes 983040 | tf_op jit(solution)/shard_map/reduce_scatter | solution.py:109
  211.1 3.5 %copy-start.7 = (f32[128,2]{0,1:T(2,128)S(1)}, f32[128,2]{0,1:T(2,128)}, u32[]{:S(2)}) copy-start(f32[128,2]{0,1:T(2,128)} %param.26) | copy-start | bytes 3076
  211.3 27.9 %copy-start.6 = (f32[2048]{0:T(1024)S(1)}, f32[2048]{0:T(1024)}, u32[]{:S(2)}) copy-start(f32[2048]{0:T(1024)} %param.23) | copy-start | bytes 24580
  246.4 2.9 %copy-start.5 = (f32[2048]{0:T(1024)S(1)}, f32[2048]{0:T(1024)}, u32[]{:S(2)}) copy-start(f32[2048]{0:T(1024)} %param.31) | copy-start | bytes 24580
Sparse Core Ops, SparseCore 0:
  62.0 45.3 all-gather.1
  128.0 58.8 reduce-scatter.4
  214.7 23.4 reduce-scatter.2
where the time goes:
time: 258 us; the launch traced here: 257 us
  blocking collectives  107 us (41%)
  waiting for transfers between devices  68.8 us (27%)
  matrix products  34.7 us (13%)
  between operations  14.1 us (5%)
  other arithmetic  13.6 us (5%)
  local copies, waits for them, and re-layouts  13.1 us (5%)
  starting transfers between devices  6.14 us (2%)
    all_gather x1, waiting for transfers between devices, expert_half(): shard_rows = lax.all_gather(flat_rows, 'tp', axis=0, tiled=True)  45.3 us
    all_to_all x1, blocking collectives, expert_half(): lax.all_to_all(outgoing, 'ep', split_axis=0, concat_axis=0, tiled=True)  44.4 us
    all_gather x1, blocking collectives, mixer_half(): key_piece = lax.all_gather(key_norm, 'ep', axis=0, tiled=True)  31.2 us
    all_gather x1, blocking collectives, mixer_half(): value_piece = lax.all_gather(values, 'ep', axis=0, tiled=True)  31 us
    reduce_scatter x1, waiting for transfers between devices, mixer_half(): lax.psum_scatter(jnp.dot(selected, out_weight, preferred_element_type=jnp...  23.4 us
    dot_general x1, matrix products, expert_half(): jnp.dot(selected, down_local, preferred_element_type=jnp.float32)  11.9 us
    dot_general x1, matrix products, expert_half(): jnp.dot(shard_rows, gate_local, preferred_element_type=jnp.float32)  8.52 us
    all_to_all x1, starting transfers between devices, expert_half(): lax.all_to_all(finished, 'ep', split_axis=0, concat_axis=0, tiled=True)  5.62 us
  transfers between devices with their start and end apart: 4, of which 2 were waited for; matrix products, arithmetic and copies ran while one was open for 8% of the time, Pallas kernels for 0%

commit v1 on v0

--- a/solution.py
+++ b/solution.py
@@ -68,8 +68,11 @@
         jnp.zeros((kv_local, group_size, local_rows), jnp.float32),
         jnp.zeros((kv_local, group_size, local_rows, HEAD), jnp.float32),
     )
-    key_piece = lax.all_gather(key_norm, "ep", axis=0, tiled=True)
-    value_piece = lax.all_gather(values, "ep", axis=0, tiled=True)
+    key_piece, value_piece = jnp.split(
+        lax.all_gather(jnp.concatenate([key_norm, values], axis=1), "ep", axis=0, tiled=True),
+        [key_norm.shape[1]],
+        axis=1,
+    )
     piece_rows = key_piece.shape[0]
     block_rows = 1
     for candidate in range(min(piece_rows, 1024), 0, -1):

time: 258 us -> 246 us (0.953)
  blocking collectives: 107 us -> 76.7 us
  waiting for transfers between devices: 68.8 us -> 87 us
    all_gather x2 -> x1, blocking collectives: 62.2 us -> 32.3 us  [mixer_half(): lax.all_gather(jnp.concatenate([key_norm, values], axis=1), 'ep', axis=0,...]
    reduce_scatter x1, waiting for transfers between devices: 0.02 us -> 11.5 us  [expert_half(): lax.psum_scatter(jnp.dot(selected, down_local, preferred_element_type=jnp...]
    all_to_all x1, waiting for transfers between devices: 0.01 us -> 6.81 us  [expert_half(): lax.all_to_all(finished, 'ep', split_axis=0, concat_axis=0, tiled=True)]
  transfers between devices with their start and end apart: 4 -> 4, of which waited for: 2 -> 4; matrix products, arithmetic and copies ran while one was open for 8% -> 8% of each run, Pallas kernels for 0% -> 0%
where the time goes in v1:
time: 246 us; the launch traced here: 245 us
  waiting for transfers between devices  87 us (35%)
  blocking collectives  76.7 us (31%)
  matrix products  34.7 us (14%)
  between operations  14.1 us (6%)
  other arithmetic  13.4 us (5%)
  local copies, waits for them, and re-layouts  13.3 us (5%)
  starting transfers between devices  6.03 us (2%)
    all_gather x1, waiting for transfers between devices, expert_half(): shard_rows = lax.all_gather(flat_rows, 'tp', axis=0, tiled=True)  45.3 us
    all_to_all x1, blocking collectives, expert_half(): lax.all_to_all(outgoing, 'ep', split_axis=0, concat_axis=0, tiled=True)  44.4 us
    all_gather x1, blocking collectives, mixer_half(): lax.all_gather(jnp.concatenate([key_norm, values], axis=1), 'ep', axis=0,...  32.3 us
    reduce_scatter x1, waiting for transfers between devices, mixer_half(): lax.psum_scatter(jnp.dot(selected, out_weight, preferred_element_type=jnp...  23.4 us
    dot_general x1, matrix products, expert_half(): jnp.dot(selected, down_local, preferred_element_type=jnp.float32)  11.9 us
    reduce_scatter x1, waiting for transfers between devices, expert_half(): lax.psum_scatter(jnp.dot(selected, down_local, preferred_element_type=jnp...  11.5 us
    dot_general x1, matrix products, expert_half(): jnp.dot(shard_rows, gate_local, preferred_element_type=jnp.float32)  8.52 us
    all_to_all x1, waiting for transfers between devices, expert_half(): lax.all_to_all(finished, 'ep', split_axis=0, concat_axis=0, tiled=True)  6.81 us
  transfers between devices with their start and end apart: 4, of which 4 were waited for; matrix products, arithmetic and copies ran while one was open for 8% of the time, Pallas kernels for 0%

profile of v1, /device:TPU:0, one launch (start us, length us, event | category | flops | bytes accessed | tf_op | source)
XLA Modules:
  0.0 245.4 jit_solution(10976174144972154664)
XLA Ops:
  10.3 1.4 scatter_custom_fusion
  11.8 1.2 fusion.25
  13.0 1.2 fusion.27
  14.3 3.1 %gather_fusion = bf16[384,2048]{1,0:T(8,128)(2,1)} fusion(bf16[129,2048]{1,0:T(8,128)(2,1)S(1)} %concatenate.49, s32[1024]{0:T(1024)S(1)} %pad_clamp_fusion.1), kind=kCustom, calls=%fused_computation | custom fusion | bytes 3147264 | tf_op jit(solution)/shard_map/gather | solution.py:141
  17.4 44.4 %all_to_all.10 = bf16[8,48,2048]{2,1,0:T(8,128)(2,1)} all-to-all(bf16[8,48,2048]{2,1,0:T(8,128)(2,1)} %bitcast.136), channel_id=1, replica_groups=mesh['ep'=8,'tp'=4] {'ep'}, dimensions={0} | all-to-all | bytes 3145728 | tf_op jit(solution)/shard_map/all_to_all | solution.py:145
  62.1 45.3 %all-gather.2.cloned.1.call-done = bf16[1536,2048]{1,0:T(8,128)(2,1)} async-done(((bf16[384,2048]{1,0:T(8,128)(2,1)}), bf16[1536,2048]{1,0:T(8,128)(2,1)}) %all-gather.2.cloned.1.call-update) | async-done | bytes 6291472 | tf_op jit(solution)/shard_map/all_gather | solution.py:147
  107.4 8.5 %convolution_minimum_fusion = f32[1536,512]{1,0:T(8,128)} fusion(bf16[1536,2048]{1,0:T(8,128)(2,1)} %all-gather.2.cloned.1.call-done, bf16[1,2048,512]{2,1,0:T(8,128)(2,1)} %param.28), kind=kOutput, calls=%fused_computation.30 | convolution fusion | flops 3222011904 | bytes 11534336 | tf_op jit(solution)/shard_map/dot_general | solution.py:149
  115.9 11.9 %convolution_convert_fusion = bf16[1536,2048]{1,0:T(8,128)(2,1)} fusion(bf16[1,512,2048]{2,1,0:T(8,128)(2,1)S(1)} %copy-done, f32[1536,512]{1,0:T(8,128)} %convolution_minimum_fusion, bf16[1536,2048]{1,0:T(8,128)(2,1)} %all-gather.2.cloned.1.call-done, bf16[1,2048,512]{2,1,0:T(8,128)(2,1)} %param.29), kind=kOutput, calls=%fused_computation.28 | convolution fusion | flops 6452674560 | bytes 19922944 | tf_op jit(solution)/shard_map/dot_general | solution.py:154
  132.9 32.3 %all_gather.6 = bf16[1536,256]{1,0:T(8,128)(2,1)S(1)} all-gather(bf16[192,256]{1,0:T(8,128)(2,1)S(1)} %concatenate.43), channel_id=1, replica_groups=mesh['ep'=8,'tp'=4] {'ep'}, dimensions={0}, use_global_device_ids=true | all-gather | bytes 884736 | tf_op jit(solution)/shard_map/all_gather | solution.py:72
  165.3 10.1 %while.15 = (s32[]{:T(128)}, f32[1,4,192]{2,1,0:T(4,128)S(1)}, f32[1,4,192]{2,1,0:T(4,128)S(1)}, f32[1,4,192,128]{3,2,1,0:T(8,128)S(1)}, bf16[2,768,1,128]{3,1,2...) while((s32[]{:T(128)}, f32[1,4,192]{2,1,0:T(4,128)S(1)}, ...), condition=%wide.region_5.6_spmd.clone, body=%wide.region_2.5_spmd.clone.sunk | while | flops 307008000 | bytes 17942668 | solution.py:104
  165.3 1.9 bitcast_reduce_fusion.2
  167.2 2.5 %fusion.95 = f32[1,4,192,128]{3,2,1,0:T(8,128)S(1)} fusion(f32[768,192,4]{0,1,2:T(8,128)} %get-tuple-element.176, f32[4,192]{1,0:T(4,128)S(1)} %bitcast.139, f32[1,4,192,128]{3,2,1,0:T(8,128)S(1)} %get-tuple-element.190, bf16[2,768,1,128]{3,1,2,0:T(8,128)(2,1)S(1)} %get-tuple-element.202, s32[]{:T(128)} %get-tuple-element.187, ...), kind=kOutput, calls=%fused_computation.9.clone.1 | convolution fusion | flops 153059328 | bytes 3350533 | tf_op jit(solution)/shard_map/while/body/eval_jaxpr/hgqk,khd->hgqd/dot_general | solution.py:96
  170.4 1.9 bitcast_reduce_fusion.2
  172.3 2.5 %fusion.95 = f32[1,4,192,128]{3,2,1,0:T(8,128)S(1)} fusion(f32[768,192,4]{0,1,2:T(8,128)} %get-tuple-element.176, f32[4,192]{1,0:T(4,128)S(1)} %bitcast.139, f32[1,4,192,128]{3,2,1,0:T(8,128)S(1)} %get-tuple-element.190, bf16[2,768,1,128]{3,1,2,0:T(8,128)(2,1)S(1)} %get-tuple-element.202, s32[]{:T(128)} %get-tuple-element.187, ...), kind=kOutput, calls=%fused_computation.9.clone.1 | convolution fusion | flops 153059328 | bytes 3350533 | tf_op jit(solution)/shard_map/while/body/eval_jaxpr/hgqk,khd->hgqd/dot_general | solution.py:96
  175.4 11.5 %reduce-scatter.5.cloned.1.call-done = bf16[384,2048]{1,0:T(8,128)(2,1)} async-done(((bf16[1536,2048]{1,0:T(8,128)(2,1)}), bf16[384,2048]{1,0:T(8,128)(2,1)}) %reduce-scatter.5.cloned.1.call-update) | async-done | bytes 1572880 | tf_op jit(solution)/shard_map/reduce_scatter | solution.py:153
  186.9 5.5 %all-to-all-start.1 = ((bf16[8,48,2048]{2,1,0:T(8,128)(2,1)}), bf16[8,48,2048]{2,1,0:T(8,128)(2,1)}, u32[]{:S(2)}, u32[]{:S(2)}) async-start(bf16[8,48,2048]{2,1,0:T(8,128)(2,1)} %bitcast.141), calls=%async_computation.3 | async-start | bytes 3145728 | tf_op jit(solution)/shard_map/all_to_all | solution.py:160
  193.0 3.1 %convolution_convert_fusion.1 = bf16[192,2048]{1,0:T(8,128)(2,1)} fusion(bf16[512,2048]{1,0:T(8,128)(2,1)} %param.22, bf16[24,8,4,128]{3,2,1,0:T(4,128)(2,1)S(1)} %bitcast.142), kind=kOutput, calls=%fused_computation.35 | convolution fusion | flops 403046400 | bytes 3080192 | tf_op jit(solution)/shard_map/dot_general | solution.py:113
  196.3 23.4 %reduce-scatter.3.cloned.1.call-done = bf16[48,2048]{1,0:T(8,128)(2,1)} async-done(((bf16[192,2048]{1,0:T(8,128)(2,1)}), bf16[48,2048]{1,0:T(8,128)(2,1)}) %reduce-scatter.3.cloned.1.call-update) | async-done | bytes 196624 | tf_op jit(solution)/shard_map/reduce_scatter | solution.py:112
  220.8 1.7 fusion.35
  222.5 6.8 %all-to-all-done.1 = bf16[8,48,2048]{2,1,0:T(8,128)(2,1)} async-done(((bf16[8,48,2048]{2,1,0:T(8,128)(2,1)}), bf16[8,48,2048]{2,1,0:T(8,128)(2,1)}, u32[]{:S(2)}, u32[]{:S(2)}) %all-to-all-start.1) | async-done | bytes 1572896 | tf_op jit(solution)/shard_map/all_to_all | solution.py:160
  229.3 4.0 %gather_fusion.1 = bf16[256,2048]{1,0:T(8,128)(2,1)S(1)} fusion(bf16[384,2048]{1,0:T(8,128)(2,1)} %bitcast.23, s32[1024]{0:T(1024)S(1)} %pad_clamp_fusion), kind=kCustom, calls=%fused_computation.1 | custom fusion | bytes 2098176 | tf_op jit(solution)/shard_map/gather | solution.py:161
  233.3 1.5 reshape.497
  234.8 2.5 %fusion.80 = f32[128,1,2048]{2,1,0:T(1,128)S(1)} fusion(bf16[128,2,2048]{2,1,0:T(2,128)(2,1)} %reshape.497, bf16[128,2,1]{1,2,0:T(2,128)(2,1)S(1)} %copy.35), kind=kOutput, calls=%fused_computation.144 | convolution fusion | flops 1048576 | bytes 2097664 | tf_op jit(solution)/shard_map/tk,tkd->td/dot_general | solution.py:164
  237.7 1.2 fusion.30
  (82 shorter events, 11.9 us)
Async XLA Ops:
  7.2 108.7 %copy-start = (bf16[1,512,2048]{2,1,0:T(8,128)(2,1)S(1)}, bf16[1,512,2048]{2,1,0:T(8,128)(2,1)}, u32[]{:S(2)}) copy-start(bf16[1,512,2048]{2,1,0:T(8,128)(2,1)} %param.30) | copy-start | bytes 6291460
  7.2 100.2 %all-gather.2.cloned.1.call-start = ((), (), s32[]{:S(2)}) async-start(), calls=%async_computation.5 | async-start | bytes 7864320 | tf_op jit(solution)/shard_map/all_gather | solution.py:147
  61.9 125.0 %reduce-scatter.5.cloned.1.call-start = ((), (), s32[]{:S(2)}) async-start(), calls=%async_computation.6 | async-start | bytes 7864320 | tf_op jit(solution)/shard_map/reduce_scatter | solution.py:153
  127.8 0.9 copy-start.3
  127.9 2.2 copy-start.8
  130.0 1.7 copy-start.2
  130.0 1.8 copy-start.9
  130.3 2.5 %copy-start.4 = (bf16[192,128]{1,0:T(8,128)(2,1)S(1)}, bf16[192,128]{1,0:T(8,128)(2,1)}, u32[]{:S(2)}) copy-start(bf16[192,128]{1,0:T(8,128)(2,1)} %param.19) | copy-start | bytes 147460
  167.2 2.5 %copy-start.1 = (f32[768,192,4]{0,1,2:T(8,128)S(1)}, f32[768,192,4]{0,1,2:T(8,128)}, u32[]{:S(2)}) copy-start(f32[768,192,4]{0,1,2:T(8,128)} %get-tuple-element.176) | copy-start | bytes 7077892 | tf_op jit(solution)/shard_map/while
  172.3 2.5 %copy-start.1 = (f32[768,192,4]{0,1,2:T(8,128)S(1)}, f32[768,192,4]{0,1,2:T(8,128)}, u32[]{:S(2)}) copy-start(f32[768,192,4]{0,1,2:T(8,128)} %get-tuple-element.176) | copy-start | bytes 7077892 | tf_op jit(solution)/shard_map/while
  186.9 42.5 %all-to-all-start.1 = ((bf16[8,48,2048]{2,1,0:T(8,128)(2,1)}), bf16[8,48,2048]{2,1,0:T(8,128)(2,1)}, u32[]{:S(2)}, u32[]{:S(2)}) async-start(bf16[8,48,2048]{2,1,0:T(8,128)(2,1)} %bitcast.141), calls=%async_computation.3 | async-start | bytes 3145728 | tf_op jit(solution)/shard_map/all_to_all | solution.py:160
  192.4 27.3 %reduce-scatter.3.cloned.1.call-start = ((), (), s32[]{:S(2)}) async-start(), calls=%async_computation.4 | async-start | bytes 983040 | tf_op jit(solution)/shard_map/reduce_scatter | solution.py:112
  192.7 3.5 %copy-start.7 = (f32[128,2]{0,1:T(2,128)S(1)}, f32[128,2]{0,1:T(2,128)}, u32[]{:S(2)}) copy-start(f32[128,2]{0,1:T(2,128)} %param.26) | copy-start | bytes 3076
  192.9 28.0 %copy-start.6 = (f32[2048]{0:T(1024)S(1)}, f32[2048]{0:T(1024)}, u32[]{:S(2)}) copy-start(f32[2048]{0:T(1024)} %param.23) | copy-start | bytes 24580
  234.8 2.9 %copy-start.5 = (f32[2048]{0:T(1024)S(1)}, f32[2048]{0:T(1024)}, u32[]{:S(2)}) copy-start(f32[2048]{0:T(1024)} %param.31) | copy-start | bytes 24580
Sparse Core Ops, SparseCore 0:
  62.0 45.3 all-gather.1
  128.0 58.8 reduce-scatter.4
  196.2 23.4 reduce-scatter.2
